TPU v7x, 32 devices: a whole 2x2x4 slice. The times are simulated.
32 devices in a mesh: sp: 4 (over y, x), dp: 8 (over z, core).
Axes of the slice: x: 2, y: 2, z: 4, core: 2. Of those that a mesh axis runs over, the one named last changes fastest.
Arguments:
- tokens: bfloat16 [8, 512, 2048], P('dp', 'sp'), may hold values from -6 to 6
- query_weight: bfloat16 [2048, 1024], P('dp'), may hold values from -0.125 to 0.125
- key_weight: bfloat16 [2048, 1024], P('dp'), may hold values from -0.125 to 0.125
- value_weight: bfloat16 [2048, 2048], P('dp'), may hold values from -0.125 to 0.125
- output_weight: bfloat16 [2048, 2048], P('dp'), may hold values from -0.125 to 0.125
- log_decay: float32 [2, 16], P(None, 'sp'), may hold values from -0.04 to 0, as said below
Outputs:
- mixed: bfloat16 [8, 512, 2048], P('dp', 'sp')
Inputs may be any that keep to these rules, and one draw needn't show every extreme that they name: `log_decay`: every entry is negative: the logarithm of a head's decay per position.
All inputs are finite; a program needn't handle non-finite values.
Results may differ from a plain program's by a relative error of at most 0.012.
Values may be sent and summed in bfloat16 or wider, within the bound.
A program may use at most 128 MiB of HBM per device.

v0:
```python
import jax
import jax.numpy as jnp
from jax import lax
from jax.sharding import PartitionSpec as P

HEADS = 16
DK = 64
DV = 128
BLOCK = 512
exact_precision = lax.Precision.HIGHEST


def rotate(values_part, positions):
    half_dim = values_part.shape[-1] // 2
    frequency = 10000.0 ** (-jnp.arange(half_dim, dtype=jnp.float32) / half_dim)
    angles = positions[:, None] * frequency[None, :]
    cosine = jnp.cos(angles)[:, None, :]
    sine_part = jnp.sin(angles)[:, None, :]
    first = values_part[..., :half_dim]
    second = values_part[..., half_dim:]
    return jnp.concatenate(
        [first * cosine - second * sine_part, first * sine_part + second * cosine], axis=-1
    )


def retain(query, key_rows, value_rows, log_rate):
    length, heads, key_dim = query.shape
    value_dim = value_rows.shape[-1]
    count = length // BLOCK
    offsets = jnp.arange(BLOCK, dtype=jnp.float32)
    distance = offsets[:, None] - offsets[None, :]
    decay_inner = jnp.where(
        distance[None] >= 0.0,
        jnp.exp(log_rate[:, None, None] * jnp.maximum(distance, 0.0)[None]),
        0.0,
    )
    decay_query = jnp.exp((offsets[:, None] + 1.0) * log_rate[None, :])[:, :, None]
    decay_key = jnp.exp((BLOCK - 1.0 - offsets)[:, None] * log_rate[None, :])[:, :, None]
    decay_block = jnp.exp(BLOCK * log_rate)[:, None, None]

    def blocks(array):
        return array.reshape(count, BLOCK, heads, array.shape[-1])

    def advance(state, inputs):
        query_block, key_block, value_block = inputs
        inner = (
            jnp.einsum("ihd,jhd->hij", query_block, key_block, preferred_element_type=jnp.float32)
            * decay_inner
        )
        result = jnp.einsum(
            "hij,jhv->ihv",
            inner.astype(jnp.bfloat16),
            value_block,
            preferred_element_type=jnp.float32,
        )
        query_wide = query_block.astype(jnp.float32) * decay_query
        result = result + jnp.einsum("ihd,hdv->ihv", query_wide, state, precision=exact_precision)
        key_wide = key_block.astype(jnp.float32) * decay_key
        state = state * decay_block + jnp.einsum(
            "jhd,jhv->hdv", key_wide, value_block.astype(jnp.float32), precision=exact_precision
        )
        return (state, result)

    initial = jnp.zeros((heads, key_dim, value_dim), jnp.float32)
    final_state, outputs = lax.scan(
        advance, initial, (blocks(query), blocks(key_rows), blocks(value_rows))
    )
    return outputs.reshape(length, heads, value_dim)


def mechanism(stacked, log_decay):
    length = stacked.shape[0]
    widened = stacked[..., : 2 * DK].astype(jnp.float32)
    positions = jnp.arange(length, dtype=jnp.float32)
    query = rotate(widened[..., :DK], positions).astype(jnp.bfloat16)
    key_rows = rotate(widened[..., DK : 2 * DK], positions).astype(jnp.bfloat16)
    value_rows = stacked[..., 2 * DK :]
    forward = retain(query, key_rows, value_rows, log_decay[0])
    backward = retain(
        jnp.flip(query, 0), jnp.flip(key_rows, 0), jnp.flip(value_rows, 0), log_decay[1]
    )
    combined = forward + jnp.flip(backward, 0)
    average = jnp.mean(combined, axis=-1, keepdims=True)
    centred = combined - average
    variance = jnp.mean(centred * centred, axis=-1, keepdims=True)
    return (centred * lax.rsqrt(variance + 1e-06)).astype(jnp.bfloat16)


def shards(tokens, query_weight, key_weight, value_weight, output_weight, log_decay):
    rows = tokens[0]
    row_count = rows.shape[0]
    local_heads = log_decay.shape[1]
    first_head = lax.axis_index("sp") * local_heads
    own_slices = jnp.concatenate(
        [
            lax.dynamic_slice_in_dim(query_weight, first_head * DK, local_heads * DK, 1),
            lax.dynamic_slice_in_dim(key_weight, first_head * DK, local_heads * DK, 1),
            lax.dynamic_slice_in_dim(value_weight, first_head * DV, local_heads * DV, 1),
        ],
        axis=1,
    )
    own_whole = lax.all_gather(own_slices, "dp", axis=0, tiled=True)
    piece = lax.all_gather(rows, "sp", axis=0, tiled=True)
    count = piece.shape[0]
    product = jnp.dot(piece, own_whole, preferred_element_type=jnp.float32).astype(jnp.bfloat16)
    query_part = product[:, : local_heads * DK].reshape(count, local_heads, DK)
    key_part = product[:, local_heads * DK : 2 * local_heads * DK].reshape(count, local_heads, DK)
    value_part = product[:, 2 * local_heads * DK :].reshape(count, local_heads, DV)
    gathered = jnp.concatenate([query_part, key_part, value_part], axis=2)
    normed = mechanism(gathered, log_decay)
    by_token = lax.all_to_all(normed, "sp", split_axis=0, concat_axis=1, tiled=True).reshape(
        row_count, HEADS * DV
    )
    mixed = jnp.dot(
        by_token,
        lax.all_gather(output_weight, "dp", axis=0, tiled=True),
        preferred_element_type=jnp.float32,
    )
    return mixed.astype(jnp.bfloat16)[None]


def solution(mesh):
    placed = (
        P("dp", "sp", None),
        P("dp", None),
        P("dp", None),
        P("dp", None),
        P("dp", None),
        P(None, "sp"),
    )
    return jax.shard_map(
        shards, mesh=mesh, in_specs=placed, out_specs=P("dp", "sp", None), check_vma=False
    )
```

profile of v0, /device:TPU:0, one launch (start us, length us, event | category | flops | bytes accessed | tf_op | source)
XLA Modules:
  0.0 190.1 jit_solution(7368320106620068643)
XLA Ops:
  6.5 0.7 all-gather.9.cloned.1.call-update
  7.3 0.0 all-gather.5.cloned.1.call-start
  7.3 0.4 copy-done
  7.8 1.0 constant_dynamic-slice_fusion.1
  8.8 0.9 pad_maximum_fusion
  9.7 0.0 all-gather.7.cloned.1.call-start
  9.7 0.7 all-gather.7.cloned.1.call-update
  10.4 1.0 fusion.15
  11.4 0.2 fusion.14
  11.6 0.1 multiply_exponential_fusion.1
  11.7 0.3 fusion.25
  12.0 35.1 %all-gather.9.cloned.1.call-done = bf16[1,512,2048]{2,1,0:T(8,128)(2,1)} async-done(((bf16[1,128,2048]{2,1,0:T(8,128)(2,1)}), bf16[1,512,2048]{2,1,0:T(8,128)(2,1)}) %all-gather.9.cloned.1.call-update) | async-done | bytes 2097168 | tf_op jit(solution)/shard_map/all_gather | solution.py:103
  47.1 48.5 %all-gather.5.cloned.1.call-done = bf16[2048,1024]{1,0:T(8,128)(2,1)} async-done(((bf16[256,1024]{1,0:T(8,128)(2,1)}), bf16[2048,1024]{1,0:T(8,128)(2,1)}) %all-gather.5.cloned.1.call-update) | async-done | bytes 4194320 | tf_op jit(solution)/shard_map/all_gather | solution.py:102
  95.6 5.2 %fusion.8 = bf16[512,1024]{0,1:T(8,128)(2,1)S(1)} fusion(bf16[2048,1024]{1,0:T(8,128)(2,1)} %all-gather.5.cloned.1.call-done, bf16[1,512,2048]{2,1,0:T(8,128)(2,1)} %all-gather.9.cloned.1.call-done), kind=kOutput, calls=%fused_computation.9 | convolution fusion | flops 2148007936 | bytes 7340032 | tf_op jit(solution)/shard_map/dot_general | solution.py:105
  101.0 0.1 maximum_convert_fusion
  101.1 0.2 subtract_convert_fusion
  101.3 1.6 rev.17
  103.0 0.5 rev.16
  103.5 5.7 %rev.15 = bf16[512,4,128]{0,2,1:T(8,128)(2,1)} reverse(bf16[512,4,128]{0,2,1:T(8,128)(2,1)S(1)} %bitcast.36), dimensions={0} | reverse | bytes 1048576 | tf_op jit(solution)/shard_map/jit(_flip)/rev | solution.py:80
  109.2 4.2 %fusion.4 = f32[4,128,512]{2,1,0:T(8,128)} fusion(bf16[512,4,128]{0,2,1:T(8,128)(2,1)} %rev.15, bf16[512,4,64]{0,2,1:T(8,128)(2,1)S(1)} %rev.16, bf16[512,4,64]{0,2,1:T(8,128)(2,1)} %rev.17, f32[4]{0:T(128)} %copy-done.5, f32[512,512]{1,0:T(8,128)S(1)} %fusion.14, pred[512,512]{1,0:T(8,128)(4,1)} %fusion.15), kind=kOutput, calls=%fused_computation.7 | convolution fusion | flops 406847488 | bytes 3407888 | tf_op jit(solution)/shard_map/while/body/eval_jaxpr/hij,jhv->ihv/dot_general | solution.py:50
  113.4 2.2 %fusion.11 = f32[512,4,128]{0,2,1:T(8,128)S(1)} fusion(f32[4,128,512]{2,1,0:T(8,128)} %fusion.4, bf16[512,4,64]{0,2,1:T(8,128)(2,1)S(1)} %rev.16, f32[512,4]{0,1:T(4,128)S(1)} %get-tuple-element.60), kind=kOutput, calls=%fused_computation.11 | convolution fusion | flops 201850880 | bytes 2367488 | tf_op jit(solution)/shard_map/while/body/eval_jaxpr/ihd,hdv->ihv/dot_general | solution.py:57
  115.6 1.5 rev.18
  117.0 3.4 %fusion.3 = f32[4,128,512]{2,1,0:T(8,128)S(1)} fusion(bf16[512,4,128]{0,2,1:T(8,128)(2,1)} %bitcast.37, f32[512,512]{1,0:T(8,128)} %copy-done.2, f32[4]{0:T(128)} %copy-done.4, pred[512,512]{1,0:T(8,128)(4,1)} %fusion.15, bf16[512,4,32]{0,2,1:T(8,128)(2,1)} %copy-done.3, bf16[512,4,32]{0,2,1:T(8,128)(2,1)S(1)} %get-tuple-element.43, ...), kind=kOutput, calls=%fused_computation.6 | convolution fusion | flops 407896064 | bytes 3407888 | tf_op jit(solution)/shard_map/while/body/eval_jaxpr/hij,jhv->ihv/dot_general | solution.py:50
  120.5 1.0 fusion.31
  121.5 0.1 multiply_reduce_fusion
  121.7 0.1 multiply_convert_fusion.2
  121.8 0.3 copy.9
  122.1 12.3 %all_to_all.15 = bf16[512,4,128]{2,1,0:T(4,128)(2,1)S(1)} all-to-all(bf16[512,4,128]{2,1,0:T(4,128)(2,1)S(1)} %copy.9), channel_id=1, replica_groups=mesh['sp'=4,'dp'=8] {'sp'}, dimensions={0} | all-to-all | bytes 1048576 | tf_op jit(solution)/shard_map/all_to_all | solution.py:111
  134.5 0.1 copy.10
  134.6 0.3 copy.11
  134.8 43.3 %all-gather.7.cloned.1.call-done = bf16[2048,2048]{1,0:T(8,128)(2,1)} async-done(((bf16[256,2048]{1,0:T(8,128)(2,1)}), bf16[2048,2048]{1,0:T(8,128)(2,1)}) %all-gather.7.cloned.1.call-update) | async-done | bytes 8388624 | tf_op jit(solution)/shard_map/all_gather | solution.py:116
  178.1 5.5 %fusion = bf16[1,128,2048]{2,1,0:T(8,128)(2,1)} fusion(bf16[128,2048]{0,1:T(8,128)(2,1)S(1)} %bitcast.35, bf16[2048,2048]{1,0:T(8,128)(2,1)} %all-gather.7.cloned.1.call-done), kind=kOutput, calls=%fused_computation.3 | convolution fusion | flops 1074003968 | bytes 9437184 | tf_op jit(solution)/shard_map/dot_general | solution.py:114
  (25 shorter events, 0.2 us)
Async XLA Ops:
  6.5 1.2 copy-start
  6.5 5.0 %copy-start.6 = (f32[2,4]{1,0:T(2,128)S(1)}, f32[2,4]{1,0:T(2,128)}, u32[]{:S(2)}) copy-start(f32[2,4]{1,0:T(2,128)} %param.11) | copy-start | bytes 100
  6.5 40.6 %all-gather.9.cloned.1.call-start = ((), (), s32[]{:S(2)}) async-start(), calls=%async_computation.3 | async-start | bytes 2621440 | tf_op jit(solution)/shard_map/all_gather | solution.py:103
  7.3 88.3 %all-gather.5.cloned.1.call-start = ((), (), s32[]{:S(2)}) async-start(), calls=%async_computation.1 | async-start | bytes 4718592 | tf_op jit(solution)/shard_map/all_gather | solution.py:102
  9.7 168.5 %all-gather.7.cloned.1.call-start = ((), (), s32[]{:S(2)}) async-start(), calls=%async_computation.2 | async-start | bytes 9437184 | tf_op jit(solution)/shard_map/all_gather | solution.py:116
  11.6 97.6 %copy-start.2 = (f32[512,512]{1,0:T(8,128)}, f32[512,512]{1,0:T(8,128)S(1)}, u32[]{:S(2)}) copy-start(f32[512,512]{1,0:T(8,128)S(1)} %fusion.14) | copy-start | bytes 3145732
  11.6 89.3 %copy-start.4 = (f32[4]{0:T(128)}, f32[4]{0:T(128)S(1)}, u32[]{:S(2)}) copy-start(f32[4]{0:T(128)S(1)} %get-tuple-element.61) | copy-start | bytes 52
  11.6 89.3 %copy-start.5 = (f32[4]{0:T(128)}, f32[4]{0:T(128)S(1)}, u32[]{:S(2)}) copy-start(f32[4]{0:T(128)S(1)} %get-tuple-element.62) | copy-start | bytes 52
  100.9 12.4 %copy-start.1 = (bf16[512,512]{0,1:T(8,128)(2,1)}, bf16[512,512]{0,1:T(8,128)(2,1)S(1)}, u32[]{:S(2)}) copy-start(bf16[512,512]{0,1:T(8,128)(2,1)S(1)} %slice.42) | copy-start | bytes 1572868
  101.3 1.7 copy-start.3
Sparse Core Ops, SparseCore 0:
  9.2 37.8 all-gather.8
  48.7 46.8 all-gather.4
  97.2 80.8 all-gather.6
where the time goes:
time: 190 us
  waiting for transfers between devices  128 us (67%)
  matrix products  21.5 us (11%)
  between operations  13.3 us (7%)
  blocking collectives  12.3 us (6%)
  local copies, waits for them, and re-layouts  11.6 us (6%)
  other arithmetic  3.01 us (2%)
    all_gather x1, waiting for transfers between devices, shards(): own_whole = lax.all_gather(own_slices, 'dp', axis=0, tiled=True)  48.5 us
    all_gather x1, waiting for transfers between devices, shards(): lax.all_gather(output_weight, 'dp', axis=0, tiled=True)  43.3 us
    all_gather x1, waiting for transfers between devices, shards(): piece = lax.all_gather(rows, 'sp', axis=0, tiled=True)  35.1 us
    all_to_all x1, blocking collectives, shards(): lax.all_to_all(normed, 'sp', split_axis=0, concat_axis=1, tiled=True)  12.3 us
    dot_general x2, matrix products, advance(): jnp.einsum('hij,jhv->ihv', inner.astype(jnp.bfloat16), value_block, prefe...  7.56 us
    rev x1, local copies, waits for them, and re-layouts, mechanism(): jnp.flip(value_rows, 0)  5.71 us
    dot_general x1, matrix products, shards(): jnp.dot(by_token, lax.all_gather(output_weight, 'dp', axis=0, tiled=True)...  5.46 us
    dot_general x1, matrix products, shards(): jnp.dot(piece, own_whole, preferred_element_type=jnp.float32)  5.25 us
  transfers between devices with their start and end apart: 3, of which 3 were waited for; matrix products, arithmetic and copies ran while one was open for 16% of the time, Pallas kernels for 0%

commit v1 on v0

--- a/solution.py
+++ b/solution.py
@@ -100,7 +100,12 @@
         axis=1,
     )
     own_whole = lax.all_gather(own_slices, "dp", axis=0, tiled=True)
-    piece = lax.all_gather(rows, "sp", axis=0, tiled=True)
+    ring = [rows]
+    for hop in range(3):
+        ring.append(lax.ppermute(ring[-1], "sp", [(dev, (dev + 1) % 4) for dev in range(4)]))
+    piece = jnp.roll(
+        jnp.concatenate(ring[::-1], axis=0), (lax.axis_index("sp") + 1) * ring[0].shape[0], axis=0
+    )
     count = piece.shape[0]
     product = jnp.dot(piece, own_whole, preferred_element_type=jnp.float32).astype(jnp.bfloat16)
     query_part = product[:, : local_heads * DK].reshape(count, local_heads, DK)

time: 190 us -> 155 us (0.82)
  waiting for transfers between devices: 128 us -> 77.3 us
  local copies, waits for them, and re-layouts: 11.6 us -> 20.4 us
  starting transfers between devices: 0.08 us -> 3.85 us
  other arithmetic: 3.01 us -> 6.75 us
    all_gather x1, waiting for transfers between devices: 48.5 us -> 0.01 us  [shards(): own_whole = lax.all_gather(own_slices, 'dp', axis=0, tiled=True)]
    ppermute x0 -> x3, waiting for transfers between devices: none -> 36.5 us  [shards(): lax.ppermute(ring[-1], 'sp', [(dev, (dev + 1) % 4) for dev in range(4)])]
    all_gather x1 -> x0, waiting for transfers between devices: 35.1 us -> none  [shards(): piece = lax.all_gather(rows, 'sp', axis=0, tiled=True)]
    unnamed x14 -> x23, local copies, waits for them, and re-layouts: 0.47 us -> 7.23 us
    ppermute x0 -> x3, starting transfers between devices: none -> 3.8 us  [shards(): lax.ppermute(ring[-1], 'sp', [(dev, (dev + 1) % 4) for dev in range(4)])]
    all_gather x1, waiting for transfers between devices: 43.3 us -> 40.1 us  [shards(): lax.all_gather(output_weight, 'dp', axis=0, tiled=True)]
  transfers between devices with their start and end apart: 3 -> 5, of which waited for: 3 -> 4; matrix products, arithmetic and copies ran while one was open for 16% -> 26% of each run, Pallas kernels for 0% -> 0%
where the time goes in v1:
time: 155 us; the launch traced here: 154 us
  waiting for transfers between devices  77.3 us (50%)
  matrix products  21.4 us (14%)
  local copies, waits for them, and re-layouts  20.4 us (13%)
  between operations  13.6 us (9%)
  blocking collectives  10.9 us (7%)
  other arithmetic  6.75 us (4%)
  starting transfers between devices  3.85 us (2%)
    all_gather x1, waiting for transfers between devices, shards(): lax.all_gather(output_weight, 'dp', axis=0, tiled=True)  40.1 us
    ppermute x3, waiting for transfers between devices, shards(): lax.ppermute(ring[-1], 'sp', [(dev, (dev + 1) % 4) for dev in range(4)])  36.5 us
    all_to_all x1, blocking collectives, shards(): lax.all_to_all(normed, 'sp', split_axis=0, concat_axis=1, tiled=True)  10.9 us
    dot_general x2, matrix products, advance(): jnp.einsum('hij,jhv->ihv', inner.astype(jnp.bfloat16), value_block, prefe...  7.6 us
    unnamed x23, local copies, waits for them, and re-layouts  7.23 us
    rev x1, local copies, waits for them, and re-layouts, mechanism(): jnp.flip(value_rows, 0)  5.71 us
    dot_general x1, matrix products, shards(): jnp.dot(by_token, lax.all_gather(output_weight, 'dp', axis=0, tiled=True)...  5.46 us
    dot_general x1, matrix products, shards(): jnp.dot(piece, own_whole, preferred_element_type=jnp.float32)  5.15 us
  transfers between devices with their start and end apart: 5, of which 4 were waited for; matrix products, arithmetic and copies ran while one was open for 26% of the time, Pallas kernels for 0%

profile of v1, /device:TPU:0, one launch (start us, length us, event | category | flops | bytes accessed | tf_op | source)
XLA Modules:
  0.0 154.2 jit_solution(15698099767894030324)
XLA Ops:
  6.6 1.2 copy-done
  7.8 1.0 constant_dynamic-slice_fusion.1
  8.8 0.9 pad_maximum_fusion
  10.4 3.0 %collective-permute-start = (bf16[128,2048]{1,0:T(8,128)(2,1)}, bf16[128,2048]{1,0:T(8,128)(2,1)S(1)}, u32[]{:S(2)}, u32[]{:S(2)}) collective-permute-start(bf16[128,2048]{1,0:T(8,128)(2,1)} %bitcast.30), channel_id=1, source_target_pairs={{0,8},{8,16},{16,24},{24,0},{1,9},{9,17},{17,25},{25,1},{2,10},{10... | collective-permute-start | bytes 1572872 | tf_op jit(solution)/shard_map/ppermute | solution.py:105
  13.5 13.1 %collective-permute-done = bf16[128,2048]{1,0:T(8,128)(2,1)S(1)} collective-permute-done((bf16[128,2048]{1,0:T(8,128)(2,1)}, bf16[128,2048]{1,0:T(8,128)(2,1)S(1)}, u32[]{:S(2)}, u32[]{:S(2)}) %collective-permute-start) | collective-permute-done | bytes 524320 | tf_op jit(solution)/shard_map/ppermute | solution.py:105
  27.3 1.0 fusion.12
  28.3 1.2 fusion.11
  29.5 11.2 %collective-permute-done.1 = bf16[128,2048]{1,0:T(8,128)(2,1)S(1)} collective-permute-done((bf16[128,2048]{1,0:T(8,128)(2,1)S(1)}, bf16[128,2048]{1,0:T(8,128)(2,1)S(1)}, u32[]{:S(2)}, u32[]{:S(2)}) %collective-permute-start.1) | collective-permute-done | bytes 524320 | tf_op jit(solution)/shard_map/ppermute | solution.py:105
  40.7 1.0 fusion.22
  41.7 12.3 %collective-permute-done.2 = bf16[128,2048]{1,0:T(8,128)(2,1)S(1)} collective-permute-done((bf16[128,2048]{1,0:T(8,128)(2,1)S(1)}, bf16[128,2048]{1,0:T(8,128)(2,1)S(1)}, u32[]{:S(2)}, u32[]{:S(2)}) %collective-permute-start.2) | collective-permute-done | bytes 524320 | tf_op jit(solution)/shard_map/ppermute | solution.py:105
  54.0 0.9 constant_dynamic-update-slice_fusion.7
  54.8 0.8 constant_dynamic-update-slice_fusion.6
  55.7 0.9 constant_dynamic-update-slice_fusion.5
  56.6 0.8 constant_dynamic-update-slice_fusion.4
  57.4 0.8 constant_dynamic-update-slice_fusion.3
  58.2 0.9 constant_dynamic-update-slice_fusion.2
  59.1 0.9 constant_dynamic-update-slice_fusion.1
  60.0 0.8 constant_dynamic-update-slice_fusion
  60.8 5.2 %fusion.5 = bf16[512,1024]{1,0:T(8,128)(2,1)S(1)} fusion(bf16[2048,1024]{1,0:T(8,128)(2,1)} %all-gather.3.cloned.1.call-done, bf16[1024,2048]{1,0:T(8,128)(2,1)} %constant_dynamic-update-slice_fusion, s32[]{:T(128)S(6)} %select_n.28), kind=kOutput, calls=%fused_computation.8 | convolution fusion | flops 2148007936 | bytes 7340036 | tf_op jit(solution)/shard_map/dot_general | solution.py:110
  66.2 0.8 copy.22
  67.3 1.3 maximum_convert_fusion
  68.6 1.1 subtract_convert_fusion
  69.7 1.6 %rev.17 = bf16[512,4,64]{0,2,1:T(8,128)(2,1)} reverse(bf16[512,4,64]{0,2,1:T(8,128)(2,1)S(1)} %pad_maximum_fusion.2), dimensions={0} | reverse | bytes 524288 | tf_op jit(solution)/shard_map/jit(_flip)/rev | solution.py:80
  71.9 5.7 %rev.15 = bf16[512,4,128]{0,2,1:T(8,128)(2,1)} reverse(bf16[512,4,128]{0,2,1:T(8,128)(2,1)S(1)} %bitcast.31), dimensions={0} | reverse | bytes 1048576 | tf_op jit(solution)/shard_map/jit(_flip)/rev | solution.py:80
  77.6 4.2 %fusion.4 = f32[4,128,512]{2,1,0:T(8,128)} fusion(bf16[512,4,128]{0,2,1:T(8,128)(2,1)} %rev.15, bf16[512,4,64]{0,2,1:T(8,128)(2,1)S(1)} %rev.16, bf16[512,4,64]{0,2,1:T(8,128)(2,1)} %rev.17, f32[4]{0:T(128)} %copy-done.6, f32[512,512]{1,0:T(8,128)S(1)} %copy-done.3, pred[512,512]{1,0:T(8,128)(4,1)} %fusion.12), kind=kOutput, calls=%fused_computation.7 | convolution fusion | flops 406847488 | bytes 3407888 | tf_op jit(solution)/shard_map/while/body/eval_jaxpr/hij,jhv->ihv/dot_general | solution.py:50
  81.8 2.2 %fusion.8 = f32[512,4,128]{0,2,1:T(8,128)S(1)} fusion(f32[4,128,512]{2,1,0:T(8,128)} %fusion.4, bf16[512,4,64]{0,2,1:T(8,128)(2,1)S(1)} %rev.16, f32[512,4]{0,1:T(4,128)S(1)} %get-tuple-element.60), kind=kOutput, calls=%fused_computation.10 | convolution fusion | flops 201850880 | bytes 2367488 | tf_op jit(solution)/shard_map/while/body/eval_jaxpr/ihd,hdv->ihv/dot_general | solution.py:57
  84.0 1.5 rev.18
  85.5 3.4 %fusion.3 = f32[4,128,512]{2,1,0:T(8,128)S(1)} fusion(bf16[512,4,128]{0,2,1:T(8,128)(2,1)} %bitcast.32, f32[512,512]{1,0:T(8,128)} %fusion.11, f32[4]{0:T(128)} %copy-done.5, pred[512,512]{1,0:T(8,128)(4,1)} %fusion.12, bf16[512,4,32]{0,2,1:T(8,128)(2,1)} %copy-done.4, bf16[512,4,32]{0,2,1:T(8,128)(2,1)S(1)} %get-tuple-element.43, ...), kind=kOutput, calls=%fused_computation.6 | convolution fusion | flops 407896064 | bytes 3407888 | tf_op jit(solution)/shard_map/while/body/eval_jaxpr/hij,jhv->ihv/dot_general | solution.py:50
  88.9 1.0 fusion.29
  90.6 10.9 %all_to_all.15 = bf16[512,4,128]{2,1,0:T(4,128)(2,1)S(1)} all-to-all(bf16[512,4,128]{2,1,0:T(4,128)(2,1)S(1)} %copy.25), channel_id=1, replica_groups=mesh['sp'=4,'dp'=8] {'sp'}, dimensions={0} | all-to-all | bytes 1048576 | tf_op jit(solution)/shard_map/all_to_all | solution.py:116
  101.8 40.1 %all-gather.5.cloned.1.call-done = bf16[2048,2048]{1,0:T(8,128)(2,1)} async-done(((bf16[256,2048]{1,0:T(8,128)(2,1)}), bf16[2048,2048]{1,0:T(8,128)(2,1)}) %all-gather.5.cloned.1.call-update) | async-done | bytes 8388624 | tf_op jit(solution)/shard_map/all_gather | solution.py:121
  141.9 5.5 %fusion = bf16[1,128,2048]{2,1,0:T(8,128)(2,1)} fusion(bf16[128,2048]{0,1:T(8,128)(2,1)S(1)} %bitcast.29, bf16[2048,2048]{1,0:T(8,128)(2,1)} %all-gather.5.cloned.1.call-done), kind=kOutput, calls=%fused_computation.3 | convolution fusion | flops 1074003968 | bytes 9437184 | tf_op jit(solution)/shard_map/dot_general | solution.py:119
  (41 shorter events, 3.6 us)
Async XLA Ops:
  6.5 1.2 copy-start
  6.5 50.0 %copy-start.1 = (bf16[1,128,2048]{2,1,0:T(8,128)(2,1)S(1)}, bf16[1,128,2048]{2,1,0:T(8,128)(2,1)}, u32[]{:S(2)}) copy-start(bf16[1,128,2048]{2,1,0:T(8,128)(2,1)} %param.6) | copy-start | bytes 1572868
  6.5 22.9 %copy-start.7 = (f32[2,4]{1,0:T(2,128)S(1)}, f32[2,4]{1,0:T(2,128)}, u32[]{:S(2)}) copy-start(f32[2,4]{1,0:T(2,128)} %param.11) | copy-start | bytes 100
  6.5 54.3 %all-gather.3.cloned.1.call-start = ((), (), s32[]{:S(2)}) async-start(), calls=%async_computation.1 | async-start | bytes 4718592 | tf_op jit(solution)/shard_map/all_gather | solution.py:102
  9.7 132.2 %all-gather.5.cloned.1.call-start = ((), (), s32[]{:S(2)}) async-start(), calls=%async_computation.2 | async-start | bytes 9437184 | tf_op jit(solution)/shard_map/all_gather | solution.py:121
  10.4 16.1 %collective-permute-start = (bf16[128,2048]{1,0:T(8,128)(2,1)}, bf16[128,2048]{1,0:T(8,128)(2,1)S(1)}, u32[]{:S(2)}, u32[]{:S(2)}) collective-permute-start(bf16[128,2048]{1,0:T(8,128)(2,1)} %bitcast.30), channel_id=1, source_target_pairs={{0,8},{8,16},{16,24},{24,0},{1,9},{9,17},{17,25},{25,1},{2,10},{10... | collective-permute-start | bytes 1572872 | tf_op jit(solution)/shard_map/ppermute | solution.py:105
  26.5 14.1 %collective-permute-start.1 = (bf16[128,2048]{1,0:T(8,128)(2,1)S(1)}, bf16[128,2048]{1,0:T(8,128)(2,1)S(1)}, u32[]{:S(2)}, u32[]{:S(2)}) collective-permute-start(bf16[128,2048]{1,0:T(8,128)(2,1)S(1)} %collective-permute-done), channel_id=1, source_target_pairs={{0,8},{8,16},{16,24},{24,0},{1,9},{9,17},{17,25},{25,1},{2,10},{10... | collective-permute-start | bytes 1572872 | tf_op jit(solution)/shard_map/ppermute | solution.py:105
  29.5 31.3 %copy-start.5 = (f32[4]{0:T(128)}, f32[4]{0:T(128)S(1)}, u32[]{:S(2)}) copy-start(f32[4]{0:T(128)S(1)} %get-tuple-element.61) | copy-start | bytes 52
  29.5 31.3 %copy-start.6 = (f32[4]{0:T(128)}, f32[4]{0:T(128)S(1)}, u32[]{:S(2)}) copy-start(f32[4]{0:T(128)S(1)} %get-tuple-element.62) | copy-start | bytes 52
  40.6 13.3 %collective-permute-start.2 = (bf16[128,2048]{1,0:T(8,128)(2,1)S(1)}, bf16[128,2048]{1,0:T(8,128)(2,1)S(1)}, u32[]{:S(2)}, u32[]{:S(2)}) collective-permute-start(bf16[128,2048]{1,0:T(8,128)(2,1)S(1)} %collective-permute-done.1), channel_id=1, source_target_pairs={{0,8},{8,16},{16,24},{24,0},{1,9},{9,17},{17,25},{25,1},{2,10},{10... | collective-permute-start | bytes 1572872 | tf_op jit(solution)/shard_map/ppermute | solution.py:105
  66.1 11.5 %copy-start.3 = (f32[512,512]{1,0:T(8,128)S(1)}, f32[512,512]{1,0:T(8,128)}, u32[]{:S(2)}) copy-start(f32[512,512]{1,0:T(8,128)} %fusion.11) | copy-start | bytes 3145732
  67.3 14.5 %copy-start.2 = (bf16[512,512]{0,1:T(8,128)(2,1)}, bf16[512,512]{0,1:T(8,128)(2,1)S(1)}, u32[]{:S(2)}) copy-start(bf16[512,512]{0,1:T(8,128)(2,1)S(1)} %copy.28) | copy-start | bytes 1572868
  69.7 1.7 %copy-start.4 = (bf16[512,4,32]{0,2,1:T(8,128)(2,1)}, bf16[512,4,32]{0,2,1:T(8,128)(2,1)S(1)}, u32[]{:S(2)}) copy-start(bf16[512,4,32]{0,2,1:T(8,128)(2,1)S(1)} %get-tuple-element.44) | copy-start | bytes 393220
Sparse Core Ops, SparseCore 0:
  9.8 49.5 all-gather.2
  61.0 80.8 all-gather.4
